TPU v7x, 256 devices: a whole 4x4x8 slice. The times are simulated.
256 devices in a mesh: sp: 32 (over z, y), tp: 8 (over x, core).
Axes of the slice: x: 4, y: 4, z: 8, core: 2. Of those that a mesh axis runs over, the one named last changes fastest.
Arguments:
- tokens: bfloat16 [4, 16384, 2048], P(None, ('sp', 'tp')), may hold values from -6 to 6
- in_gain: float32 [2048], replicated, may hold values from 0.1 to 1.9
- query_weight: bfloat16 [2048, 1024], P(None, 'tp'), may hold values from -0.125 to 0.125
- key_weight: bfloat16 [2048, 1024], P(None, 'tp'), may hold values from -0.125 to 0.125
- value_weight: bfloat16 [2048, 1024], P(None, 'tp'), may hold values from -0.125 to 0.125
- gate_weight: bfloat16 [2048, 1024], P(None, 'tp'), may hold values from -0.125 to 0.125
- log_decay: float32 [8], P('tp'), may hold values from -0.034 to 0, as said below
- norm_gain: float32 [1024], P('tp'), may hold values from 0.1 to 1.9
- out_weight: bfloat16 [1024, 2048], replicated, may hold values from -0.1875 to 0.1875
- post_gain: float32 [2048], replicated, may hold values from 0.1 to 1.9
Outputs:
- mixed: bfloat16 [4, 16384, 2048], P(None, ('sp', 'tp'))
Inputs may be any that keep to these rules, and one draw needn't show every extreme that they name: `log_decay`: every entry is negative; some heads keep a tenth or more of their memory over 16384 positions, others lose most of it within 30 to 100 positions.
All inputs are finite; a program needn't handle non-finite values.
Results may differ from a plain program's by a relative error of at most 0.015.
Values may be sent and summed in bfloat16 or wider, within the bound.
A program may use at most 64 MiB of HBM per device.

v0:
```python
import jax
import jax.numpy as jnp
from jax import lax
from jax.sharding import Mesh
from jax.sharding import PartitionSpec as P

HEAD_DIM = 128
BLOCK = 128
SP = ("sp_0", "sp_1")
SP_TP = ("sp_0", "sp_1", "tp")
rms_eps = 1e-06
group_eps = 1e-05
rope_base = 10000.0


def neutral_like(shard, identity):
    return jax.tree.map(
        lambda part, zero: jnp.zeros_like(part) + jnp.asarray(zero, part.dtype), shard, identity
    )


def entering(shard, axes, combine, identity):
    before = start = neutral_like(shard, identity)
    running = shard
    for axis in reversed(axes):
        length, mine = (lax.axis_size(axis), lax.axis_index(axis))
        pieces = jax.tree.map(lambda part: lax.all_gather(part, axis), running)
        inside, running = (start, start)
        for k in range(length):
            passed = k < mine
            running = combine(running, jax.tree.map(lambda part: part[k], pieces))
            inside = jax.tree.map(lambda new, old: jnp.where(passed, new, old), running, inside)
        before = combine(inside, before)
    return before


def rotate(values, positions):
    half_dim = values.shape[-1] // 2
    inverse = rope_base ** (-jnp.arange(half_dim, dtype=jnp.float32) / half_dim)
    angles = positions.astype(jnp.float32)[:, None] * inverse[None, :]
    cosine = jnp.cos(angles)
    sine_part = jnp.sin(angles)
    first_half = values[..., :half_dim].astype(jnp.float32)
    second = values[..., half_dim:].astype(jnp.float32)
    return jnp.concatenate(
        [first_half * cosine - second * sine_part, first_half * sine_part + second * cosine],
        axis=-1,
    )


def local_pass(queries, key_rows, values, log_decay):
    seq_count, head_count, length, head_width = queries.shape
    block_count = length // BLOCK
    offsets = jnp.arange(BLOCK, dtype=jnp.float32)
    distance = offsets[:, None] - offsets[None, :]
    rate_col = log_decay[:, None, None]
    inside = jnp.where(distance >= 0, jnp.exp(rate_col * jnp.maximum(distance, 0.0)), 0.0)
    query_scale = jnp.exp(log_decay[:, None] * (offsets + 1.0))[..., None]
    key_scale = jnp.exp(log_decay[:, None] * (BLOCK - 1.0 - offsets))[..., None]
    block_decay = jnp.exp(log_decay * BLOCK)[:, None, None]

    def to_blocks(arr):
        return arr.reshape(seq_count, head_count, block_count, BLOCK, arr.shape[-1]).transpose(
            2, 0, 1, 3, 4
        )

    def advance(memory, inputs):
        q_block, k_block, v_block = inputs
        scores = jnp.einsum("shqd,shkd->shqk", q_block, k_block, preferred_element_type=jnp.float32)
        weights = (scores * inside).astype(jnp.bfloat16)
        within = jnp.einsum("shqk,shkv->shqv", weights, v_block, preferred_element_type=jnp.float32)
        carried = jnp.einsum("shqd,shdv->shqv", q_block.astype(jnp.float32) * query_scale, memory)
        k_scaled = (k_block.astype(jnp.float32) * key_scale).astype(jnp.bfloat16)
        memory = memory * block_decay + jnp.einsum(
            "shkd,shkv->shdv", k_scaled, v_block, preferred_element_type=jnp.float32
        )
        return (memory, within + carried)

    start_memory = jnp.zeros((seq_count, head_count, head_width, values.shape[-1]), jnp.float32)
    end_state, outputs = lax.scan(
        advance, start_memory, (to_blocks(queries), to_blocks(key_rows), to_blocks(values))
    )
    outputs = outputs.transpose(1, 2, 0, 3, 4).reshape(
        seq_count, head_count, length, values.shape[-1]
    )
    return (outputs, end_state)


def combine(earlier, later_part):
    return (
        earlier[0] * later_part[0],
        earlier[1] * later_part[0][None, :, None, None] + later_part[1],
    )


def read_out(carried, queries, partial_out, log_decay):
    length = queries.shape[2]
    read_scale = jnp.exp(log_decay[:, None] * (jnp.arange(length, dtype=jnp.float32) + 1.0))[
        ..., None
    ]
    return partial_out + jnp.einsum(
        "shld,shdv->shlv", queries.astype(jnp.float32) * read_scale, carried
    )


def body(
    tokens,
    in_gain,
    query_weight,
    key_weight,
    value_weight,
    gate_weight,
    log_decay,
    norm_gain,
    out_weight,
    post_gain,
):
    seq_count, rows_dev, model_width = tokens.shape
    tp_size = lax.axis_size("tp")
    local_width = query_weight.shape[1]
    head_count = local_width // HEAD_DIM
    stretch = rows_dev * tp_size
    tok_f32 = tokens.astype(jnp.float32)
    normed = (
        tok_f32 * lax.rsqrt(jnp.mean(tok_f32 * tok_f32, axis=-1, keepdims=True) + rms_eps) * in_gain
    ).astype(jnp.bfloat16)
    joined = jnp.concatenate([query_weight, key_weight, value_weight, gate_weight], axis=1)
    projected = jnp.einsum(
        "kux,xt->kut",
        lax.all_gather(normed, "tp", axis=1, tiled=True),
        joined,
        preferred_element_type=jnp.float32,
    ).astype(jnp.bfloat16)

    def heads_of(columns):
        return columns.reshape(seq_count, stretch, head_count, HEAD_DIM).transpose(0, 2, 1, 3)

    positions = lax.axis_index(SP) * stretch + jnp.arange(stretch, dtype=jnp.int32)
    queries = rotate(heads_of(projected[..., :local_width]), positions).astype(jnp.bfloat16)
    key_rows = (
        rotate(heads_of(projected[..., local_width : 2 * local_width]), positions)
        * HEAD_DIM ** (-0.5)
    ).astype(jnp.bfloat16)
    values = heads_of(projected[..., 2 * local_width : 3 * local_width])
    gating = projected[..., 3 * local_width :]
    partial_out, end_state = local_pass(queries, key_rows, values, log_decay)
    span_decay = jnp.exp(log_decay * stretch)
    carried = entering(
        (span_decay, end_state), SP, combine, (jnp.ones_like(span_decay), jnp.zeros_like(end_state))
    )[1]
    retained = read_out(carried, queries, partial_out, log_decay)
    center = jnp.mean(retained, axis=-1, keepdims=True)
    spread = jnp.mean(jnp.square(retained - center), axis=-1, keepdims=True)
    normal = (
        ((retained - center) * lax.rsqrt(spread + group_eps))
        .transpose(0, 2, 1, 3)
        .reshape(seq_count, stretch, local_width)
    )
    gated = (normal * norm_gain * jax.nn.silu(gating.astype(jnp.float32))).astype(jnp.bfloat16)
    premix = jnp.einsum(
        "hor,rn->hon",
        lax.all_to_all(gated, "tp", split_axis=1, concat_axis=2, tiled=True),
        out_weight,
        preferred_element_type=jnp.float32,
    )
    mixed = (
        premix * lax.rsqrt(jnp.mean(premix * premix, axis=-1, keepdims=True) + rms_eps) * post_gain
    )
    return mixed.astype(jnp.bfloat16)


def solution(mesh):
    torus = Mesh(mesh.devices.reshape(8, 4, mesh.shape["tp"]), ("sp_0", "sp_1", "tp"))
    return jax.shard_map(
        body,
        mesh=torus,
        in_specs=(
            P(None, SP_TP, None),
            P(),
            P(None, "tp"),
            P(None, "tp"),
            P(None, "tp"),
            P(None, "tp"),
            P("tp"),
            P("tp"),
            P(),
            P(),
        ),
        out_specs=P(None, SP_TP, None),
        check_vma=False,
    )
```

profile of v0, /device:TPU:1, one launch (start us, length us, event | category | flops | bytes accessed | tf_op | source)
XLA Modules:
  0.0 204.7 jit_solution(9332395953188734523)
XLA Ops:
  6.5 1.6 fusion.44
  8.1 2.6 %fusion.46 = bf16[4,64,2048]{2,1,0:T(8,128)(2,1)} fusion(bf16[4,64,2048]{2,1,0:T(8,128)(2,1)} %param.12, f32[2048]{0:T(1024)} %param.13, f32[4,64]{1,0:T(4,128)S(1)} %add_rsqrt_fusion.2), kind=kLoop, calls=%fused_computation.48 | loop fusion | flops 2097152 | bytes 2106368 | tf_op jit(solution)/shard_map/convert_element_type | solution.py:126
  10.9 0.2 copy.39
  11.1 0.2 copy.40
  11.3 0.5 copy-done.10
  11.8 0.2 copy.41
  12.0 0.2 copy.42
  13.0 0.5 multiply_cosine_fusion
  13.5 53.8 %all-gather.7.cloned.1.call-done = bf16[4,512,2048]{2,1,0:T(8,128)(2,1)} async-done(((bf16[4,64,2048]{2,1,0:T(8,128)(2,1)}), bf16[4,512,2048]{2,1,0:T(8,128)(2,1)}) %all-gather.7.cloned.1.call-update) | async-done | bytes 8388624 | tf_op jit(solution)/shard_map/all_gather | solution.py:130
  67.3 9.5 %fusion.54 = bf16[4,512,512]{1,2,0:T(8,128)(2,1)S(1)} fusion(bf16[4,512,2048]{2,1,0:T(8,128)(2,1)} %all-gather.7.cloned.1.call-done, bf16[2048,128]{0,1:T(8,128)(2,1)S(1)} %copy.42, bf16[2048,128]{0,1:T(8,128)(2,1)S(1)} %copy.41, bf16[2048,128]{0,1:T(8,128)(2,1)S(1)} %copy.40, bf16[2048,128]{0,1:T(8,128)(2,1)S(1)} %copy.39), kind=kOutput, calls=%fused_computation.59 | convolution fusion | flops 4304404480 | bytes 12582912 | tf_op jit(solution)/shard_map/kux,xt->kut/dot_general | solution.py:128
  76.9 1.0 slice_bitcast_fusion
  77.9 0.3 fusion.66
  78.4 0.3 copy.46
  78.8 0.3 copy-done.6
  79.3 0.3 copy.47
  79.8 0.3 copy.43
  80.3 1.3 copy.44
  81.6 1.2 reshape_transpose_reshape.3
  82.8 0.4 copy.45
  83.2 0.3 maximum_bitcast_fusion.4
  83.5 0.9 copy-done.1
  84.4 0.3 fusion.69
  84.8 11.9 %while.15 = (s32[]{:T(128)}, f32[4,1,128,128]{3,2,0,1:T(8,128)S(1)}, f32[4,4,1,128,128]{4,3,1,2,0:T(8,128)}, f32[1]{0:T(128)}, bf16[4,4,1,128,128]{4,3,1,2,0:T(8...) while((s32[]{:T(128)}, ...), condition=%wide.region_2.3_spmd.clone.clone.clone, body=%wide.region_1.2_spmd.clone.clone.clone.sunk | while | flops 67977728 | bytes 2496632 | solution.py:80
  84.8 0.7 select_bitcast_fusion.2
  85.5 0.3 fusion.146
  85.9 0.7 exponential_bitcast_fusion.3
  86.5 0.9 fusion.147
  87.5 0.3 fusion.145
  87.8 0.7 select_bitcast_fusion.2
  88.5 0.3 fusion.146
  88.8 0.7 exponential_bitcast_fusion.3
  89.5 0.9 fusion.147
  90.4 0.3 fusion.145
  90.8 0.7 select_bitcast_fusion.2
  91.5 0.3 fusion.146
  91.8 0.7 exponential_bitcast_fusion.3
  92.5 0.9 fusion.147
  93.4 0.3 fusion.145
  93.8 0.7 select_bitcast_fusion.2
  94.5 0.3 fusion.146
  94.8 0.7 exponential_bitcast_fusion.3
  95.5 0.9 fusion.147
  96.4 0.3 fusion.145
  96.8 0.7 copy-done
  97.5 0.6 dynamic-slice
  98.1 0.7 exponential_dynamic-update-slice_fusion
  98.8 8.4 %all-reduce = f32[4]{0:T(128)S(1)} all-reduce(f32[4]{0:T(128)S(1)} %exponential_dynamic-update-slice_fusion), channel_id=2, replica_groups=mesh['sp_0'=8,'sp_1'=4,'tp'=8] {'sp_1'}, use_global_device_ids=true, to_apply=%add | all-reduce | flops 4 | bytes 32
  107.2 0.7 slice_multiply_fusion.1
  107.9 1.3 slice_multiply_fusion
  109.9 12.2 %all-gather.11.cloned.1.call-done = f32[16,1,128,128]{3,2,1,0:T(8,128)} async-done(((f32[4,1,128,128]{3,2,1,0:T(8,128)}), f32[16,1,128,128]{3,2,1,0:T(8,128)}) %all-gather.11.cloned.1.call-update) | async-done | bytes 1048592 | tf_op jit(solution)/shard_map/all_gather | solution.py:27
  122.0 3.8 %slice_add_fusion.8 = f32[4,1,128,128]{3,2,1,0:T(8,128)} fusion(f32[16,1,128,128]{3,2,1,0:T(8,128)} %all-gather.11.cloned.1.call-done, f32[]{:T(128)} %bitcast.20, f32[]{:T(128)} %bitcast.18, f32[16,1,128,128]{3,2,0,1:T(8,128)} %bitcast.197, f32[]{:T(128)} %bitcast.16, f32[]{:T(128)} %bitcast.13), kind=kLoop, calls=%fused_computation.109 | loop fusion | flops 458752 | bytes 1310736 | tf_op jit(solution)/shard_map/add | solution.py:92
  125.9 0.6 dynamic-slice.1
  126.4 1.3 dynamic-update-slice.1
  127.7 13.9 %all-reduce.1 = f32[8]{0:T(128)S(1)} all-reduce(f32[8]{0:T(128)S(1)} %dynamic-update-slice.1), channel_id=3, replica_groups=mesh['sp_0'=8,'sp_1'=4,'tp'=8] {'sp_0'}, use_global_device_ids=true, to_apply=%add.1 | all-reduce | flops 8 | bytes 64
  141.6 0.7 fusion.127
  145.5 0.4 copy.48
  145.9 0.4 reshape.499
  146.3 18.7 %all-gather.9.cloned.1.call-done = f32[8,4,1,128,128]{4,3,2,1,0:T(8,128)} async-done(((f32[1,4,1,128,128]{4,3,2,1,0:T(8,128)}), f32[8,4,1,128,128]{4,3,2,1,0:T(8,128)}) %all-gather.9.cloned.1.call-update) | async-done | bytes 2097168 | tf_op jit(solution)/shard_map/all_gather | solution.py:27
  165.1 7.9 %fusion.128 = (f32[4,512]{1,0:T(4,128)S(1)}, f32[4,512,128]{1,2,0:T(8,128)S(1)}) fusion(f32[4,512,128]{1,2,0:T(8,128)S(1)} %reshape.499, f32[8,4,1,128,128]{4,3,1,2,0:T(8,128)} %bitcast.204, f32[4,1,128,128]{3,2,1,0:T(8,128)S(1)} %copy-done.4, f32[16,1,128,128]{3,2,0,1:T(8,128)S(1)} %bitcast.198, f32[16,1,128,128]{3,2,1,0:T(8,128)S(1)} %copy-done.3, ...), kind=kOutput, calls=%fused_computation.175 | convolution fusion | flops 71170048 | bytes 5777468 | tf_op jit(solution)/shard_map/shld,shdv->shlv/dot_general | solution.py:101
  173.2 1.5 fusion.62
  174.7 0.3 copy.65
  175.0 18.3 %all_to_all.18 = bf16[4,512,128]{2,0,1:T(4,128)(2,1)S(1)} all-to-all(bf16[4,512,128]{2,0,1:T(4,128)(2,1)S(1)} %copy.65), channel_id=1, replica_groups=mesh['sp_0'=8,'sp_1'=4,'tp'=8] {'tp'}, dimensions={1} | all-to-all | bytes 1048576 | tf_op jit(solution)/shard_map/all_to_all | solution.py:162
  193.4 3.6 %multiply_reduce_fusion = (f32[4,64]{1,0:T(4,128)S(1)}, f32[4,64,2048]{2,1,0:T(8,128)S(1)}) fusion(bf16[1024,2048]{1,0:T(8,128)(2,1)} %param.20, bf16[4,8,8,8,128]{4,3,2,1,0:T(8,128)(2,1)S(1)} %bitcast.203), kind=kOutput, calls=%fused_computation.58 | convolution fusion | flops 1074790144 | bytes 6816768 | tf_op jit(solution)/shard_map/hor,rn->hon/dot_general | solution.py:160
  197.0 1.2 multiply_convert_fusion.2
  (51 shorter events, 1.3 us)
Async XLA Ops:
  6.5 4.3 %copy-start.8 = (bf16[2048,128]{1,0:T(8,128)(2,1)S(1)}, bf16[2048,128]{1,0:T(8,128)(2,1)}, u32[]{:S(2)}) copy-start(bf16[2048,128]{1,0:T(8,128)(2,1)} %param.14) | copy-start | bytes 1572868
  6.5 60.8 %all-gather.7.cloned.1.call-start = ((), (), s32[]{:S(2)}) async-start(), calls=%async_computation.1 | async-start | bytes 9437184 | tf_op jit(solution)/shard_map/all_gather | solution.py:130
  8.1 3.0 %copy-start.9 = (bf16[2048,128]{1,0:T(8,128)(2,1)S(1)}, bf16[2048,128]{1,0:T(8,128)(2,1)}, u32[]{:S(2)}) copy-start(bf16[2048,128]{1,0:T(8,128)(2,1)} %param.15) | copy-start | bytes 1572868
  10.8 1.0 copy-start.10
  10.8 1.3 copy-start.11
  10.8 111.2 %all-gather.11.cloned.1.call-start = ((), (), s32[]{:S(2)}) async-start(), calls=%async_computation.3 | async-start | bytes 1310720 | tf_op jit(solution)/shard_map/all_gather | solution.py:27
  76.9 1.5 copy-start.2
  78.3 0.7 copy-start.6
  78.4 0.8 copy-start.7
  83.2 1.2 copy-start.1
  84.8 12.8 %copy-start.15 = (u32[256]{0:T(256)S(1)}, u32[256]{0:T(256)}, u32[]{:S(2)}) copy-start(u32[256]{0:T(256)} %constant.86) | copy-start | bytes 3076
  84.8 41.1 %copy-start.14 = (u32[256]{0:T(256)S(1)}, u32[256]{0:T(256)}, u32[]{:S(2)}) copy-start(u32[256]{0:T(256)} %constant.91) | copy-start | bytes 3076
  96.7 0.7 copy-start
  96.7 48.7 %copy-start.5 = (f32[4,4,1,128,128]{4,3,1,2,0:T(8,128)S(1)}, f32[4,4,1,128,128]{4,3,1,2,0:T(8,128)}, u32[]{:S(2)}) copy-start(f32[4,4,1,128,128]{4,3,1,2,0:T(8,128)} %get-tuple-element.58) | copy-start | bytes 3145732
  97.5 67.6 %all-gather.9.cloned.1.call-start = ((), (), s32[]{:S(2)}) async-start(), calls=%async_computation.2 | async-start | bytes 2359296 | tf_op jit(solution)/shard_map/all_gather | solution.py:27
  145.5 19.6 %copy-start.3 = (f32[16,1,128,128]{3,2,1,0:T(8,128)S(1)}, f32[16,1,128,128]{3,2,1,0:T(8,128)}, u32[]{:S(2)}) copy-start(f32[16,1,128,128]{3,2,1,0:T(8,128)} %all-gather.11.cloned.1.call-done) | copy-start | bytes 3145732
  145.5 19.6 %copy-start.4 = (f32[4,1,128,128]{3,2,1,0:T(8,128)S(1)}, f32[4,1,128,128]{3,2,1,0:T(8,128)}, u32[]{:S(2)}) copy-start(f32[4,1,128,128]{3,2,1,0:T(8,128)} %slice_add_fusion.8) | copy-start | bytes 786436
  165.1 8.1 %copy-start.13 = (f32[128]{0:T(128)S(1)}, f32[128]{0:T(128)}, u32[]{:S(2)}) copy-start(f32[128]{0:T(128)} %param.19) | copy-start | bytes 1540
  193.4 3.6 %copy-start.12 = (f32[2048]{0:T(1024)S(1)}, f32[2048]{0:T(1024)}, u32[]{:S(2)}) copy-start(f32[2048]{0:T(1024)} %param.21) | copy-start | bytes 24580
Sparse Core Ops, SparseCore 0:
  10.9 56.3 all-gather.6
  97.6 24.3 all-gather.10
  126.0 39.0 all-gather.8
where the time goes:
time: 205 us
  waiting for transfers between devices  84.8 us (41%)
  blocking collectives  40.6 us (20%)
  matrix products  27.4 us (13%)
  other arithmetic  20.4 us (10%)
  between operations  18 us (9%)
  local copies, waits for them, and re-layouts  13.3 us (6%)
    all_gather x1, waiting for transfers between devices, body(): lax.all_gather(normed, 'tp', axis=1, tiled=True)  53.8 us
    all_gather x2, waiting for transfers between devices, entering(): pieces = jax.tree.map(lambda part: lax.all_gather(part, axis), running)  30.9 us
    unnamed x2, blocking collectives  22.3 us
    all_to_all x1, blocking collectives, body(): lax.all_to_all(gated, 'tp', split_axis=1, concat_axis=2, tiled=True)  18.3 us
    dot_general x1, matrix products, body(): jnp.einsum('kux,xt->kut', lax.all_gather(normed, 'tp', axis=1, tiled=True...  9.51 us
    dot_general x1, matrix products, read_out(): jnp.einsum('shld,shdv->shlv', queries.astype(jnp.float32) * read_scale, c...  7.93 us
    unnamed x41, local copies, waits for them, and re-layouts  6.03 us
  transfers between devices with their start and end apart: 3, of which 3 were waited for; matrix products, arithmetic and copies ran while one was open for 4% of the time, Pallas kernels for 0%

commit v1 on v0

--- a/solution.py
+++ b/solution.py
@@ -3,6 +3,7 @@
 from jax import lax
 from jax.sharding import Mesh
 from jax.sharding import PartitionSpec as P
+from jax.lax import axis_index, axis_size, ppermute
 
 HEAD_DIM = 128
 BLOCK = 128
@@ -115,6 +116,34 @@
     out_weight,
     post_gain,
 ):
+
+    def assign_modes(buf, state):
+        block_last, current_block, right_arr = (axis_size("tp"), axis_index("tp"), buf.shape[1])
+        pieces_in = [(ix, (ix + 1) % block_last) for ix in range(block_last)]
+        ledger = [(pp, tick) for tick, pp in pieces_in]
+        piece_now = ppermute(buf, axis_name="tp", perm=pieces_in)
+        field_out, extra = (piece_now, ppermute(buf, axis_name="tp", perm=ledger))
+        prior = state(buf, current_block * right_arr)
+        tile_out = prior.shape[1]
+        wide_out = jnp.zeros(
+            (*prior.shape[:1], block_last * tile_out, *prior.shape[2:]), prior.dtype
+        )
+
+        def check_ticks(wide_out, prior, carry_out):
+            return lax.dynamic_update_slice_in_dim(wide_out, prior, carry_out * tile_out, axis=1)
+
+        wide_out = check_ticks(wide_out, prior, current_block)
+        for num in range(1, block_last // 2 + 1):
+            reached, tmp = ((current_block - num) % block_last, (current_block + num) % block_last)
+            next_value = (field_out, extra)
+            if num < block_last // 2:
+                all_values = ppermute(field_out, axis_name="tp", perm=pieces_in)
+                field_out, extra = (all_values, ppermute(extra, perm=ledger, axis_name="tp"))
+            wide_out = check_ticks(wide_out, state(next_value[0], reached * right_arr), reached)
+            if 2 * num < block_last:
+                wide_out = check_ticks(wide_out, state(next_value[1], tmp * right_arr), tmp)
+        return wide_out
+
     seq_count, rows_dev, model_width = tokens.shape
     tp_size = lax.axis_size("tp")
     local_width = query_weight.shape[1]
@@ -125,11 +154,11 @@
         tok_f32 * lax.rsqrt(jnp.mean(tok_f32 * tok_f32, axis=-1, keepdims=True) + rms_eps) * in_gain
     ).astype(jnp.bfloat16)
     joined = jnp.concatenate([query_weight, key_weight, value_weight, gate_weight], axis=1)
-    projected = jnp.einsum(
-        "kux,xt->kut",
-        lax.all_gather(normed, "tp", axis=1, tiled=True),
-        joined,
-        preferred_element_type=jnp.float32,
+    projected = assign_modes(
+        normed,
+        state=lambda shard_2, start_2: jnp.einsum(
+            "kux,xt->kut", shard_2, joined, preferred_element_type=jnp.float32
+        ),
     ).astype(jnp.bfloat16)
 
     def heads_of(columns):

time: 205 us -> 237 us (1.16)
  waiting for transfers between devices: 84.8 us -> 43.6 us
  local copies, waits for them, and re-layouts: 13.3 us -> 45 us
  matrix products: 27.4 us -> 51.4 us
  starting transfers between devices: 0.09 us -> 15.2 us
    all_gather x1 -> x0, waiting for transfers between devices: 53.8 us -> none  [body(): lax.all_gather(normed, 'tp', axis=1, tiled=True)]
    dynamic_update_slice x0 -> x8, local copies, waits for them, and re-layouts: none -> 26.6 us  [check_ticks(): lax.dynamic_update_slice_in_dim(wide_out, prior, carry_out * tile_out, ax...]
    dot_general x1 -> x8, matrix products: 9.51 us -> 25.2 us  [body(): jnp.einsum('kux,xt->kut', shard_2, joined, preferred_element_type=jnp.flo...]
    ppermute x0 -> x7, starting transfers between devices: none -> 15.1 us  [the longest x2 6.82 us: assign_modes(): ppermute(extra, perm=ledger, axis_name='tp')]
    ppermute x0 -> x7, waiting for transfers between devices: none -> 11.8 us  [the longest x1 11.1 us: assign_modes(): piece_now = ppermute(buf, axis_name='tp', perm=pieces_in)]
    concatenate x8, local copies, waits for them, and re-layouts: 2.8 us -> 7.57 us  [rotate(): jnp.concatenate([first_half * cosine - second * sine_part, first_half * s...]
    dot_general x4, matrix products: 1.27 us -> 5.14 us  [advance(): jnp.einsum('shkd,shkv->shdv', k_scaled, v_block, preferred_element_type=j...]
    dot_general x4, matrix products: 1.33 us -> 5.19 us  [advance(): jnp.einsum('shqk,shkv->shqv', weights, v_block, preferred_element_type=jn...]
  transfers between devices with their start and end apart: 3 -> 9, of which waited for: 3 -> 4; matrix products, arithmetic and copies ran while one was open for 4% -> 23% of each run, Pallas kernels for 0% -> 0%
where the time goes in v1:
time: 237 us; the launch traced here: 235 us
  matrix products  51.4 us (22%)
  local copies, waits for them, and re-layouts  45 us (19%)
  waiting for transfers between devices  43.6 us (18%)
  blocking collectives  39 us (16%)
  other arithmetic  22.7 us (10%)
  between operations  18.4 us (8%)
  starting transfers between devices  15.2 us (6%)
    all_gather x2, waiting for transfers between devices, entering(): pieces = jax.tree.map(lambda part: lax.all_gather(part, axis), running)  31.8 us
    dynamic_update_slice x8, local copies, waits for them, and re-layouts, check_ticks(): lax.dynamic_update_slice_in_dim(wide_out, prior, carry_out * tile_out, ax...  26.6 us
    dot_general x8, matrix products, body(): jnp.einsum('kux,xt->kut', shard_2, joined, preferred_element_type=jnp.flo...  25.2 us
    unnamed x2, blocking collectives  20.7 us
    all_to_all x1, blocking collectives, body(): lax.all_to_all(gated, 'tp', split_axis=1, concat_axis=2, tiled=True)  18.3 us
    ppermute x1, waiting for transfers between devices, assign_modes(): piece_now = ppermute(buf, axis_name='tp', perm=pieces_in)  11.1 us
    dot_general x1, matrix products, read_out(): jnp.einsum('shld,shdv->shlv', queries.astype(jnp.float32) * read_scale, c...  8.53 us
    concatenate x8, local copies, waits for them, and re-layouts, rotate(): jnp.concatenate([first_half * cosine - second * sine_part, first_half * s...  7.57 us
  transfers between devices with their start and end apart: 9, of which 4 were waited for; matrix products, arithmetic and copies ran while one was open for 23% of the time, Pallas kernels for 0%

profile of v1, /device:TPU:1, one launch (start us, length us, event | category | flops | bytes accessed | tf_op | source)
XLA Modules:
  0.0 235.4 jit_solution(9119376822354365042)
XLA Ops:
  6.5 1.6 fusion.44
  8.2 1.5 fusion.46
  9.7 2.6 %collective-permute-start = (bf16[4,64,2048]{2,1,0:T(8,128)(2,1)S(1)}, bf16[4,64,2048]{2,1,0:T(8,128)(2,1)}, u32[]{:S(2)}, u32[]{:S(2)}) collective-permute-start(bf16[4,64,2048]{2,1,0:T(8,128)(2,1)S(1)} %fusion.46), channel_id=1, source_target_pairs={{0,1},{1,2},{2,3},{3,4},{4,5},{5,6},{6,7},{7,0},{8,9},{9,10},{10,1... | collective-permute-start | bytes 3145736 | tf_op jit(solution)/shard_map/ppermute | solution.py:124
  13.0 11.1 %collective-permute-done = bf16[4,64,2048]{2,1,0:T(8,128)(2,1)} collective-permute-done((bf16[4,64,2048]{2,1,0:T(8,128)(2,1)S(1)}, bf16[4,64,2048]{2,1,0:T(8,128)(2,1)}, u32[]{:S(2)}, u32[]{:S(2)}) %collective-permute-start) | collective-permute-done | bytes 1048608 | tf_op jit(solution)/shard_map/ppermute | solution.py:124
  24.1 2.6 %collective-permute-start.2 = (bf16[4,64,2048]{2,1,0:T(8,128)(2,1)}, bf16[4,64,2048]{2,1,0:T(8,128)(2,1)}, u32[]{:S(2)}, u32[]{:S(2)}) collective-permute-start(bf16[4,64,2048]{2,1,0:T(8,128)(2,1)} %collective-permute-done), channel_id=1, source_target_pairs={{0,1},{1,2},{2,3},{3,4},{4,5},{5,6},{6,7},{7,0},{8,9},{9,10},{10,1... | collective-permute-start | bytes 3145736 | tf_op jit(solution)/shard_map/ppermute | solution.py:140
  27.4 3.1 %fusion.125 = bf16[4,64,512]{1,2,0:T(8,128)(2,1)} fusion(bf16[4,64,2048]{2,1,0:T(8,128)(2,1)S(1)} %fusion.46, bf16[2048,128]{1,0:T(8,128)(2,1)S(1)} %copy-done.6, bf16[2048,128]{1,0:T(8,128)(2,1)S(1)} %copy-done.8, bf16[2048,128]{1,0:T(8,128)(2,1)S(1)} %copy-done.10, bf16[2048,128]{1,0:T(8,128)(2,1)} %param.14), kind=kOutput, calls=%fused_computation.172 | convolution fusion | flops 545259520 | bytes 3407872 | tf_op jit(solution)/shard_map/kux,xt->kut/dot_general | solution.py:159
  30.7 5.9 %dynamic_update_slice.28 = bf16[4,512,512]{1,2,0:T(8,128)(2,1)S(1)} dynamic-update-slice(bf16[4,512,512]{1,2,0:T(8,128)(2,1)S(1)} %broadcast_in_dim.10, bf16[4,64,512]{1,2,0:T(8,128)(2,1)} %fusion.125, s32[]{:T(128)} %constant.96.clone.1, s32[]{:T(128)S(6)} %select_n.211, s32[]{:T(128)} %constant.96.clone.1) | dynamic-update-slice | bytes 524292 | tf_op jit(solution)/shard_map/dynamic_update_slice | solution.py:133
  36.7 0.8 collective-permute-start.3
  38.7 2.5 %collective-permute-start.4 = (bf16[4,64,2048]{2,1,0:T(8,128)(2,1)}, bf16[4,64,2048]{2,1,0:T(8,128)(2,1)}, u32[]{:S(2)}, u32[]{:S(2)}) collective-permute-start(bf16[4,64,2048]{2,1,0:T(8,128)(2,1)} %collective-permute-done.2), channel_id=1, source_target_pairs={{0,1},{1,2},{2,3},{3,4},{4,5},{5,6},{6,7},{7,0},{8,9},{9,10},{10,1... | collective-permute-start | bytes 3145736 | tf_op jit(solution)/shard_map/ppermute | solution.py:140
  41.2 3.1 %fusion.124 = bf16[4,64,512]{1,2,0:T(8,128)(2,1)S(1)} fusion(bf16[4,64,2048]{2,1,0:T(8,128)(2,1)} %collective-permute-done, bf16[2048,128]{1,0:T(8,128)(2,1)} %param.17, bf16[2048,128]{1,0:T(8,128)(2,1)} %param.16, bf16[2048,128]{1,0:T(8,128)(2,1)} %param.15, bf16[2048,128]{1,0:T(8,128)(2,1)} %param.14), kind=kOutput, calls=%fused_computation.171 | convolution fusion | flops 545259520 | bytes 3407872 | tf_op jit(solution)/shard_map/kux,xt->kut/dot_general | solution.py:159
  44.3 2.0 dynamic_update_slice.29
  46.3 3.1 %fusion.123 = bf16[4,64,512]{1,2,0:T(8,128)(2,1)S(1)} fusion(bf16[4,64,2048]{2,1,0:T(8,128)(2,1)} %collective-permute-done.1, bf16[2048,128]{1,0:T(8,128)(2,1)} %param.17, bf16[2048,128]{1,0:T(8,128)(2,1)} %param.16, bf16[2048,128]{1,0:T(8,128)(2,1)} %param.15, bf16[2048,128]{1,0:T(8,128)(2,1)} %param.14), kind=kOutput, calls=%fused_computation.170 | convolution fusion | flops 545259520 | bytes 3407872 | tf_op jit(solution)/shard_map/kux,xt->kut/dot_general | solution.py:159
  49.5 2.0 dynamic_update_slice.30
  51.6 6.0 %collective-permute-start.5 = (bf16[4,64,2048]{2,1,0:T(8,128)(2,1)}, bf16[4,64,2048]{2,1,0:T(8,128)(2,1)}, u32[]{:S(2)}, u32[]{:S(2)}) collective-permute-start(bf16[4,64,2048]{2,1,0:T(8,128)(2,1)} %collective-permute-done.3), channel_id=1, source_target_pairs={{1,0},{2,1},{3,2},{4,3},{5,4},{6,5},{7,6},{0,7},{9,8},{10,9},{11,1... | collective-permute-start | bytes 3145736 | tf_op jit(solution)/shard_map/ppermute | solution.py:141
  57.6 3.1 %fusion.122 = bf16[4,64,512]{1,2,0:T(8,128)(2,1)S(1)} fusion(bf16[4,64,2048]{2,1,0:T(8,128)(2,1)} %collective-permute-done.2, bf16[2048,128]{1,0:T(8,128)(2,1)} %param.17, bf16[2048,128]{1,0:T(8,128)(2,1)} %param.16, bf16[2048,128]{1,0:T(8,128)(2,1)} %param.15, bf16[2048,128]{1,0:T(8,128)(2,1)} %param.14), kind=kOutput, calls=%fused_computation.169 | convolution fusion | flops 545259520 | bytes 3407872 | tf_op jit(solution)/shard_map/kux,xt->kut/dot_general | solution.py:159
  60.8 3.3 %fusion.121 = bf16[4,64,512]{1,2,0:T(8,128)(2,1)} fusion(bf16[4,64,2048]{2,1,0:T(8,128)(2,1)} %collective-permute-done.3, bf16[2048,128]{1,0:T(8,128)(2,1)S(1)} %copy-done.7, bf16[2048,128]{1,0:T(8,128)(2,1)S(1)} %copy-done.9, bf16[2048,128]{1,0:T(8,128)(2,1)S(1)} %copy-done.11, bf16[2048,128]{1,0:T(8,128)(2,1)S(1)} %copy-done.12), kind=kOutput, calls=%fused_computation.168 | convolution fusion | flops 545259520 | bytes 3407872 | tf_op jit(solution)/shard_map/kux,xt->kut/dot_general | solution.py:159
  64.1 3.3 %dynamic_update_slice.31 = bf16[4,512,512]{1,2,0:T(8,128)(2,1)S(1)} dynamic-update-slice(bf16[4,512,512]{1,2,0:T(8,128)(2,1)S(1)} %dynamic_update_slice.30, bf16[4,64,512]{1,2,0:T(8,128)(2,1)S(1)} %fusion.122, s32[]{:T(128)} %constant.96.clone.1, s32[]{:T(128)S(6)} %select_n.217, s32[]{:T(128)} %constant.96.clone.1) | dynamic-update-slice | bytes 524292 | tf_op jit(solution)/shard_map/dynamic_update_slice | solution.py:133
  67.5 5.7 %dynamic_update_slice.32 = bf16[4,512,512]{1,2,0:T(8,128)(2,1)S(1)} dynamic-update-slice(bf16[4,512,512]{1,2,0:T(8,128)(2,1)S(1)} %dynamic_update_slice.31, bf16[4,64,512]{1,2,0:T(8,128)(2,1)} %fusion.121, s32[]{:T(128)} %constant.96.clone.1, s32[]{:T(128)S(6)} %select_n.219, s32[]{:T(128)} %constant.96.clone.1) | dynamic-update-slice | bytes 524292 | tf_op jit(solution)/shard_map/dynamic_update_slice | solution.py:133
  73.2 3.1 %fusion.120 = bf16[4,64,512]{1,2,0:T(8,128)(2,1)S(1)} fusion(bf16[4,64,2048]{2,1,0:T(8,128)(2,1)} %collective-permute-done.4, bf16[2048,128]{1,0:T(8,128)(2,1)} %param.17, bf16[2048,128]{1,0:T(8,128)(2,1)} %param.16, bf16[2048,128]{1,0:T(8,128)(2,1)} %param.15, bf16[2048,128]{1,0:T(8,128)(2,1)} %param.14), kind=kOutput, calls=%fused_computation.167 | convolution fusion | flops 545259520 | bytes 3407872 | tf_op jit(solution)/shard_map/kux,xt->kut/dot_general | solution.py:159
  76.3 1.9 dynamic_update_slice.33
  78.3 3.1 %fusion.119 = bf16[4,64,512]{1,2,0:T(8,128)(2,1)S(1)} fusion(bf16[4,64,2048]{2,1,0:T(8,128)(2,1)} %collective-permute-done.5, bf16[2048,128]{1,0:T(8,128)(2,1)} %param.17, bf16[2048,128]{1,0:T(8,128)(2,1)} %param.16, bf16[2048,128]{1,0:T(8,128)(2,1)} %param.15, bf16[2048,128]{1,0:T(8,128)(2,1)} %param.14), kind=kOutput, calls=%fused_computation.166 | convolution fusion | flops 545259520 | bytes 3407872 | tf_op jit(solution)/shard_map/kux,xt->kut/dot_general | solution.py:159
  81.4 2.0 dynamic_update_slice.34
  83.4 3.1 %fusion.118 = bf16[4,64,512]{1,2,0:T(8,128)(2,1)S(1)} fusion(bf16[4,64,2048]{2,1,0:T(8,128)(2,1)} %collective-permute-done.6, bf16[2048,128]{1,0:T(8,128)(2,1)} %param.17, bf16[2048,128]{1,0:T(8,128)(2,1)} %param.16, bf16[2048,128]{1,0:T(8,128)(2,1)} %param.15, bf16[2048,128]{1,0:T(8,128)(2,1)} %param.14), kind=kOutput, calls=%fused_computation.165 | convolution fusion | flops 545259520 | bytes 3407872 | tf_op jit(solution)/shard_map/kux,xt->kut/dot_general | solution.py:159
  86.6 3.7 %dynamic_update_slice.35 = bf16[4,512,512]{1,2,0:T(8,128)(2,1)S(1)} dynamic-update-slice(bf16[4,512,512]{1,2,0:T(8,128)(2,1)S(1)} %dynamic_update_slice.34, bf16[4,64,512]{1,2,0:T(8,128)(2,1)S(1)} %fusion.118, s32[]{:T(128)} %constant.96.clone.1, s32[]{:T(128)S(6)} %select_n.225, s32[]{:T(128)} %constant.96.clone.1) | dynamic-update-slice | bytes 524292 | tf_op jit(solution)/shard_map/dynamic_update_slice | solution.py:133
  90.3 0.9 slice_bitcast_fusion
  91.2 1.4 fusion.58
  92.9 1.0 concatenate.50
  93.9 1.1 copy.59
  95.0 1.2 concatenate.46
  96.2 1.3 copy.55
  97.6 1.2 concatenate.47
  98.8 1.3 copy.56
  100.1 1.2 reshape_transpose_reshape.3
  101.3 1.1 copy.57
  102.4 1.4 maximum_bitcast_fusion.1
  103.9 2.4 %fusion.61 = bf16[4,4,1,128,128]{4,3,1,2,0:T(8,128)(2,1)} fusion(f32[4,1,4,128,64]{4,3,0,1,2:T(8,128)S(1)} %copy-done.1, f32[4,1,4,128,64]{4,3,0,1,2:T(8,128)} %copy.55), kind=kLoop, calls=%fused_computation.79 | loop fusion | flops 786432 | bytes 1572864 | tf_op jit(solution)/shard_map/transpose | solution.py:64
  106.2 19.7 %while.15 = (s32[]{:T(128)}, f32[4,1,128,128]{3,2,0,1:T(8,128)S(1)}, f32[4,4,1,128,128]{4,3,1,2,0:T(8,128)}, f32[1]{0:T(128)}, bf16[4,4,1,128,128]{4,3,1,2,0:T(8...) while((s32[]{:T(128)}, ...), condition=%wide.region_2.3_spmd.clone.clone.clone, body=%wide.region_1.2_spmd.clone.clone.clone.sunk | while | flops 67977728 | bytes 2496632 | solution.py:81
  106.2 0.7 select_bitcast_fusion.2
  107.0 1.3 fusion.152
  108.9 0.9 fusion.153
  109.9 1.3 fusion.151
  111.9 1.3 fusion.152
  113.8 0.9 fusion.153
  114.8 1.3 fusion.151
  116.8 1.3 fusion.152
  118.8 0.9 fusion.153
  119.7 1.3 fusion.151
  121.7 1.3 fusion.152
  123.7 0.9 fusion.153
  124.6 1.3 fusion.151
  127.4 0.7 exponential_dynamic-update-slice_fusion
  128.1 7.0 %all-reduce = f32[4]{0:T(128)S(1)} all-reduce(f32[4]{0:T(128)S(1)} %exponential_dynamic-update-slice_fusion), channel_id=2, replica_groups=mesh['sp_0'=8,'sp_1'=4,'tp'=8] {'sp_1'}, use_global_device_ids=true, to_apply=%add | all-reduce | flops 4 | bytes 32
  135.7 1.3 slice_multiply_fusion
  137.6 15.1 %all-gather.8.cloned.1.call-done = f32[16,1,128,128]{3,2,1,0:T(8,128)} async-done(((f32[4,1,128,128]{3,2,1,0:T(8,128)}), f32[16,1,128,128]{3,2,1,0:T(8,128)}) %all-gather.8.cloned.1.call-update) | async-done | bytes 1048592 | tf_op jit(solution)/shard_map/all_gather | solution.py:28
  152.7 3.9 %slice_add_fusion.8 = f32[4,1,128,128]{3,2,1,0:T(8,128)} fusion(f32[16,1,128,128]{3,2,1,0:T(8,128)} %all-gather.8.cloned.1.call-done, f32[]{:T(128)} %bitcast.20, f32[]{:T(128)} %bitcast.18, f32[16,1,128,128]{3,2,0,1:T(8,128)} %bitcast.209, f32[]{:T(128)} %bitcast.16, f32[]{:T(128)} %bitcast.13), kind=kLoop, calls=%fused_computation.101 | loop fusion | flops 458752 | bytes 1310736 | tf_op jit(solution)/shard_map/add | solution.py:93
  157.3 1.3 dynamic-update-slice.1
  158.6 13.7 %all-reduce.1 = f32[8]{0:T(128)S(1)} all-reduce(f32[8]{0:T(128)S(1)} %dynamic-update-slice.1), channel_id=3, replica_groups=mesh['sp_0'=8,'sp_1'=4,'tp'=8] {'sp_0'}, use_global_device_ids=true, to_apply=%add.1 | all-reduce | flops 8 | bytes 64
  176.1 1.7 copy.60
  177.8 1.4 reshape.499
  179.2 16.7 %all-gather.6.cloned.1.call-done = f32[8,4,1,128,128]{4,3,2,1,0:T(8,128)} async-done(((f32[1,4,1,128,128]{4,3,2,1,0:T(8,128)}), f32[8,4,1,128,128]{4,3,2,1,0:T(8,128)}) %all-gather.6.cloned.1.call-update) | async-done | bytes 2097168 | tf_op jit(solution)/shard_map/all_gather | solution.py:28
  195.9 8.5 %fusion.127 = (f32[4,512]{1,0:T(4,128)S(1)}, f32[4,512,128]{1,2,0:T(8,128)S(1)}) fusion(f32[4,512,128]{1,2,0:T(8,128)} %reshape.499, f32[8,4,1,128,128]{4,3,1,2,0:T(8,128)} %bitcast.216, f32[4,1,128,128]{3,2,1,0:T(8,128)S(1)} %copy-done.2, f32[16,1,128,128]{3,2,0,1:T(8,128)} %bitcast.210, f32[16,1,128,128]{3,2,1,0:T(8,128)} %all-gather.8.cloned.1.call-done, ...), kind=kOutput, calls=%fused_computation.174 | convolution fusion | flops 71170048 | bytes 5785608 | tf_op jit(solution)/shard_map/shld,shdv->shlv/dot_general | solution.py:102
  205.4 18.3 %all_to_all.18 = bf16[4,512,128]{2,0,1:T(4,128)(2,1)S(1)} all-to-all(bf16[4,512,128]{2,0,1:T(4,128)(2,1)S(1)} %copy.77), channel_id=1, replica_groups=mesh['sp_0'=8,'sp_1'=4,'tp'=8] {'tp'}, dimensions={1} | all-to-all | bytes 1048576 | tf_op jit(solution)/shard_map/all_to_all | solution.py:191
  223.7 3.6 %multiply_reduce_fusion = (f32[4,64]{1,0:T(4,128)S(1)}, f32[4,64,2048]{2,1,0:T(8,128)S(1)}) fusion(bf16[1024,2048]{1,0:T(8,128)(2,1)} %param.20, bf16[4,8,8,8,128]{4,3,2,1,0:T(8,128)(2,1)S(1)} %bitcast.215), kind=kOutput, calls=%fused_computation.51 | convolution fusion | flops 1074790144 | bytes 6816768 | tf_op jit(solution)/shard_map/hor,rn->hon/dot_general | solution.py:189
  227.3 1.2 multiply_convert_fusion.2
  (72 shorter events, 11.6 us)
Async XLA Ops:
  6.5 20.9 %copy-start.10 = (bf16[2048,128]{1,0:T(8,128)(2,1)S(1)}, bf16[2048,128]{1,0:T(8,128)(2,1)}, u32[]{:S(2)}) copy-start(bf16[2048,128]{1,0:T(8,128)(2,1)} %param.15) | copy-start | bytes 1572868
  6.5 20.9 %copy-start.8 = (bf16[2048,128]{1,0:T(8,128)(2,1)S(1)}, bf16[2048,128]{1,0:T(8,128)(2,1)}, u32[]{:S(2)}) copy-start(bf16[2048,128]{1,0:T(8,128)(2,1)} %param.16) | copy-start | bytes 1572868
  6.5 20.9 %copy-start.6 = (bf16[2048,128]{1,0:T(8,128)(2,1)S(1)}, bf16[2048,128]{1,0:T(8,128)(2,1)}, u32[]{:S(2)}) copy-start(bf16[2048,128]{1,0:T(8,128)(2,1)} %param.17) | copy-start | bytes 1572868
  6.5 146.2 %all-gather.8.cloned.1.call-start = ((), (), s32[]{:S(2)}) async-start(), calls=%async_computation.2 | async-start | bytes 1310720 | tf_op jit(solution)/shard_map/all_gather | solution.py:28
  9.7 14.3 %collective-permute-start = (bf16[4,64,2048]{2,1,0:T(8,128)(2,1)S(1)}, bf16[4,64,2048]{2,1,0:T(8,128)(2,1)}, u32[]{:S(2)}, u32[]{:S(2)}) collective-permute-start(bf16[4,64,2048]{2,1,0:T(8,128)(2,1)S(1)} %fusion.46), channel_id=1, source_target_pairs={{0,1},{1,2},{2,3},{3,4},{4,5},{5,6},{6,7},{7,0},{8,9},{9,10},{10,1... | collective-permute-start | bytes 3145736 | tf_op jit(solution)/shard_map/ppermute | solution.py:124
  12.3 24.4 %collective-permute-start.1 = (bf16[4,64,2048]{2,1,0:T(8,128)(2,1)S(1)}, bf16[4,64,2048]{2,1,0:T(8,128)(2,1)}, u32[]{:S(2)}, u32[]{:S(2)}) collective-permute-start(bf16[4,64,2048]{2,1,0:T(8,128)(2,1)S(1)} %fusion.46), channel_id=1, source_target_pairs={{1,0},{2,1},{3,2},{4,3},{5,4},{6,5},{7,6},{0,7},{9,8},{10,9},{11,1... | collective-permute-start | bytes 3145736 | tf_op jit(solution)/shard_map/ppermute | solution.py:125
  24.1 14.6 %collective-permute-start.2 = (bf16[4,64,2048]{2,1,0:T(8,128)(2,1)}, bf16[4,64,2048]{2,1,0:T(8,128)(2,1)}, u32[]{:S(2)}, u32[]{:S(2)}) collective-permute-start(bf16[4,64,2048]{2,1,0:T(8,128)(2,1)} %collective-permute-done), channel_id=1, source_target_pairs={{0,1},{1,2},{2,3},{3,4},{4,5},{5,6},{6,7},{7,0},{8,9},{9,10},{10,1... | collective-permute-start | bytes 3145736 | tf_op jit(solution)/shard_map/ppermute | solution.py:140
  36.7 14.9 %collective-permute-start.3 = (bf16[4,64,2048]{2,1,0:T(8,128)(2,1)}, bf16[4,64,2048]{2,1,0:T(8,128)(2,1)}, u32[]{:S(2)}, u32[]{:S(2)}) collective-permute-start(bf16[4,64,2048]{2,1,0:T(8,128)(2,1)} %collective-permute-done.1), channel_id=1, source_target_pairs={{1,0},{2,1},{3,2},{4,3},{5,4},{6,5},{7,6},{0,7},{9,8},{10,9},{11,1... | collective-permute-start | bytes 3145736 | tf_op jit(solution)/shard_map/ppermute | solution.py:141
  38.7 22.0 %collective-permute-start.4 = (bf16[4,64,2048]{2,1,0:T(8,128)(2,1)}, bf16[4,64,2048]{2,1,0:T(8,128)(2,1)}, u32[]{:S(2)}, u32[]{:S(2)}) collective-permute-start(bf16[4,64,2048]{2,1,0:T(8,128)(2,1)} %collective-permute-done.2), channel_id=1, source_target_pairs={{0,1},{1,2},{2,3},{3,4},{4,5},{5,6},{6,7},{7,0},{8,9},{9,10},{10,1... | collective-permute-start | bytes 3145736 | tf_op jit(solution)/shard_map/ppermute | solution.py:140
  51.5 9.3 %copy-start.7 = (bf16[2048,128]{1,0:T(8,128)(2,1)S(1)}, bf16[2048,128]{1,0:T(8,128)(2,1)}, u32[]{:S(2)}) copy-start(bf16[2048,128]{1,0:T(8,128)(2,1)} %param.17) | copy-start | bytes 1572868
  51.5 9.3 %copy-start.9 = (bf16[2048,128]{1,0:T(8,128)(2,1)S(1)}, bf16[2048,128]{1,0:T(8,128)(2,1)}, u32[]{:S(2)}) copy-start(bf16[2048,128]{1,0:T(8,128)(2,1)} %param.16) | copy-start | bytes 1572868
  51.5 9.3 %copy-start.11 = (bf16[2048,128]{1,0:T(8,128)(2,1)S(1)}, bf16[2048,128]{1,0:T(8,128)(2,1)}, u32[]{:S(2)}) copy-start(bf16[2048,128]{1,0:T(8,128)(2,1)} %param.15) | copy-start | bytes 1572868
  51.5 9.3 %copy-start.12 = (bf16[2048,128]{1,0:T(8,128)(2,1)S(1)}, bf16[2048,128]{1,0:T(8,128)(2,1)}, u32[]{:S(2)}) copy-start(bf16[2048,128]{1,0:T(8,128)(2,1)} %param.14) | copy-start | bytes 1572868
  51.6 26.7 %collective-permute-start.5 = (bf16[4,64,2048]{2,1,0:T(8,128)(2,1)}, bf16[4,64,2048]{2,1,0:T(8,128)(2,1)}, u32[]{:S(2)}, u32[]{:S(2)}) collective-permute-start(bf16[4,64,2048]{2,1,0:T(8,128)(2,1)} %collective-permute-done.3), channel_id=1, source_target_pairs={{1,0},{2,1},{3,2},{4,3},{5,4},{6,5},{7,6},{0,7},{9,8},{10,9},{11,1... | collective-permute-start | bytes 3145736 | tf_op jit(solution)/shard_map/ppermute | solution.py:141
  60.7 22.7 %collective-permute-start.6 = (bf16[4,64,2048]{2,1,0:T(8,128)(2,1)}, bf16[4,64,2048]{2,1,0:T(8,128)(2,1)}, u32[]{:S(2)}, u32[]{:S(2)}) collective-permute-start(bf16[4,64,2048]{2,1,0:T(8,128)(2,1)} %collective-permute-done.4), channel_id=1, source_target_pairs={{0,1},{1,2},{2,3},{3,4},{4,5},{5,6},{6,7},{7,0},{8,9},{9,10},{10,1... | collective-permute-start | bytes 3145736 | tf_op jit(solution)/shard_map/ppermute | solution.py:140
  92.5 2.5 %copy-start.3 = (bf16[4,1,512,64]{2,3,0,1:T(8,128)(2,1)}, bf16[4,1,512,64]{2,3,0,1:T(8,128)(2,1)S(1)}, u32[]{:S(2)}) copy-start(bf16[4,1,512,64]{2,3,0,1:T(8,128)(2,1)S(1)} %get-tuple-element.166) | copy-start | bytes 786436
  102.4 1.4 copy-start.1
  106.2 20.5 %copy-start.14 = (u32[256]{0:T(256)S(1)}, u32[256]{0:T(256)}, u32[]{:S(2)}) copy-start(u32[256]{0:T(256)} %constant.134) | copy-start | bytes 3076
  106.2 50.4 %copy-start.13 = (u32[256]{0:T(256)S(1)}, u32[256]{0:T(256)}, u32[]{:S(2)}) copy-start(u32[256]{0:T(256)} %constant.139) | copy-start | bytes 3076
  125.9 0.7 copy-start
  126.6 69.2 %all-gather.6.cloned.1.call-start = ((), (), s32[]{:S(2)}) async-start(), calls=%async_computation.1 | async-start | bytes 2359296 | tf_op jit(solution)/shard_map/all_gather | solution.py:28
  176.1 19.8 %copy-start.2 = (f32[4,1,128,128]{3,2,1,0:T(8,128)S(1)}, f32[4,1,128,128]{3,2,1,0:T(8,128)}, u32[]{:S(2)}) copy-start(f32[4,1,128,128]{3,2,1,0:T(8,128)} %slice_add_fusion.8) | copy-start | bytes 786436
  195.9 8.7 %copy-start.5 = (f32[128]{0:T(128)S(1)}, f32[128]{0:T(128)}, u32[]{:S(2)}) copy-start(f32[128]{0:T(128)} %param.19) | copy-start | bytes 1540
  223.7 3.6 %copy-start.4 = (f32[2048]{0:T(1024)S(1)}, f32[2048]{0:T(1024)}, u32[]{:S(2)}) copy-start(f32[2048]{0:T(1024)} %param.21) | copy-start | bytes 24580
Sparse Core Ops, SparseCore 0:
  126.8 25.9 all-gather.7
  156.8 39.0 all-gather.5
